TPU v7x, 32 devices: a whole 2x2x4 slice. The times are simulated.
32 devices in a mesh: sp: 4 (over z), tp: 8 (over y, x, core).
Axes of the slice: x: 2, y: 2, z: 4, core: 2. Of those that a mesh axis runs over, the one named last changes fastest.
Arguments:
- activations: bfloat16 [1024, 2048], P('sp', 'tp'), may hold values from -170 to 170
- norm_gain: float32 [2048], replicated, may hold values from 0.1 to 1.9
- query_weight: bfloat16 [2048, 1536], P(None, 'tp'), may hold values from -0.125 to 0.125
- latent_weight: bfloat16 [2048, 512], P(None, 'tp'), may hold values from -0.125 to 0.125
- rope_key_weight: bfloat16 [2048, 64], replicated, may hold values from -0.125 to 0.125
- latent_gain: float32 [512], replicated, may hold values from 1.5 to 64
- expand_weight: bfloat16 [512, 2048], P(None, 'tp'), may hold values from -0.25 to 0.25
- gate_weight: bfloat16 [2048, 1024], P(None, 'tp'), may hold values from -0.125 to 0.125
- pre_weight: bfloat16 [2048, 1024], P(None, 'tp'), may hold values from -0.125 to 0.125
- value_weight: bfloat16 [2048, 1024], P(None, 'tp'), may hold values from -0.125 to 0.125
- conv_kernel: bfloat16 [3, 1024], P(None, 'tp'), may hold values from -3.5 to 3.5
- output_attend: bfloat16 [1024, 2048], P('tp'), may hold values from -0.1875 to 0.1875
- output_conv: bfloat16 [1024, 2048], P('tp'), may hold values from -0.125 to 0.125
Outputs:
- mixed: bfloat16 [1024, 2048], P(('sp', 'tp'))
- log_weight_sum: float32 [8, 1024], P('tp', 'sp')
All inputs are finite; a program needn't handle non-finite values.
Results may differ from a plain program's by a relative error of at most 0.035.
The roundings to bfloat16 on the way count: a program that leaves them out, or rounds other values in their place, can miss the bound.
Values may be sent and summed in bfloat16 or wider, within the bound.
A program may use at most 128 MiB of HBM per device.

v0:
```python
import math
import jax
import jax.numpy as jnp
from jax import lax
from jax.sharding import PartitionSpec as P

D = 2048
NOPE = 128
ROPE = 64
VDIM = 128
GRID_W = 64
EPSILON = 1e-06
ROPE_BASE = 10000.0


def with_halo(array, sides, width):
    for axis, dim in sides:
        peers, length = (lax.axis_size(axis), array.shape[dim])
        up = [(i, (i + 1) % peers) for i in range(peers - 1)]
        down = [(j, i) for i, j in up]
        last = lax.slice_in_dim(array, length - width, length, axis=dim)
        leading = lax.slice_in_dim(array, 0, width, axis=dim)
        before = lax.ppermute(last, axis, up)
        after = lax.ppermute(leading, axis, down)
        array = jnp.concatenate([before, array, after], axis=dim)
    return array


def rotate(inputs, grid_rows, grid_cols):
    quarter = inputs.shape[-1] // 4
    inverse = ROPE_BASE ** (-jnp.arange(quarter, dtype=jnp.float32) / quarter)
    row_angle = (grid_rows[:, None] * inverse)[:, None, :]
    col_angle = (grid_cols[:, None] * inverse)[:, None, :]
    part_one = inputs[..., :quarter]
    part_two = inputs[..., quarter : 2 * quarter]
    part_three = inputs[..., 2 * quarter : 3 * quarter]
    part_four = inputs[..., 3 * quarter :]
    return jnp.concatenate(
        [
            part_one * jnp.cos(row_angle) - part_two * jnp.sin(row_angle),
            part_one * jnp.sin(row_angle) + part_two * jnp.cos(row_angle),
            part_three * jnp.cos(col_angle) - part_four * jnp.sin(col_angle),
            part_three * jnp.sin(col_angle) + part_four * jnp.cos(col_angle),
        ],
        axis=-1,
    )


def conv_branch(gate_proj, pre_proj, value_proj, conv_kernel):
    pre_mix = (pre_proj * value_proj).astype(jnp.bfloat16)
    padded = with_halo(pre_mix, (("sp", 0),), 1).astype(jnp.float32)
    kernel = conv_kernel.astype(jnp.float32)
    convolved = kernel[0] * padded[:-2] + kernel[1] * padded[1:-1] + kernel[2] * padded[2:]
    return (gate_proj * convolved).astype(jnp.bfloat16)


def body(
    activations,
    norm_gain,
    query_weight,
    latent_weight,
    rope_key_weight,
    latent_gain,
    expand_weight,
    gate_weight,
    pre_weight,
    value_weight,
    conv_kernel,
    output_attend,
    output_conv,
):
    tokens_here = activations.shape[0]
    query_cols = query_weight.shape[1]
    heads_here = query_cols // (NOPE + ROPE)
    latent_cols = latent_weight.shape[1]
    channels = gate_weight.shape[1]
    joined = jnp.concatenate(
        [query_weight, latent_weight, rope_key_weight, gate_weight, pre_weight, value_weight],
        axis=1,
    )
    inputs_f32 = activations.astype(jnp.float32)
    squares = lax.psum(jnp.sum(inputs_f32 * inputs_f32, axis=1, keepdims=True), "tp")
    partial_squares = jnp.zeros((tokens_here, 1), jnp.float32)
    piece_f32 = lax.all_gather(activations, "tp", axis=1, tiled=True).astype(jnp.float32)
    scaled = (piece_f32 * norm_gain).astype(jnp.bfloat16)
    running = jnp.dot(scaled, joined, preferred_element_type=jnp.float32)
    running, folded_squares = (running, partial_squares)
    inv_rms = lax.rsqrt(squares / D + EPSILON)
    projected = running * inv_rms
    latent_end = query_cols + latent_cols
    rope_end = latent_end + ROPE
    query_proj = projected[:, :query_cols]
    latent_proj = projected[:, query_cols:latent_end]
    rope_proj = projected[:, latent_end:rope_end]
    gate_proj = projected[:, rope_end : rope_end + channels]
    pre_proj = projected[:, rope_end + channels : rope_end + 2 * channels]
    value_proj = projected[:, rope_end + 2 * channels :]
    positions = lax.axis_index("sp") * tokens_here + jnp.arange(tokens_here, dtype=jnp.int32)
    grid_rows = (positions // GRID_W).astype(jnp.float32)
    grid_cols = (positions % GRID_W).astype(jnp.float32)
    query = query_proj.reshape(tokens_here, heads_here, NOPE + ROPE)
    query = jnp.concatenate(
        [query[..., :NOPE], rotate(query[..., NOPE:], grid_rows, grid_cols)], axis=-1
    )
    query = (query * (NOPE + ROPE) ** (-0.5)).astype(jnp.bfloat16)
    query_nope = query[..., :NOPE]
    query_rope = query[..., NOPE:]
    gathered = lax.all_gather(latent_proj.astype(jnp.bfloat16), "tp", axis=1, tiled=True).astype(
        jnp.float32
    )
    latent = (
        gathered
        * lax.rsqrt(jnp.mean(gathered * gathered, axis=1, keepdims=True) + EPSILON)
        * latent_gain
    ).astype(jnp.bfloat16)
    expanded = jnp.dot(latent, expand_weight, preferred_element_type=jnp.float32).astype(
        jnp.bfloat16
    )
    rope_key = rotate(rope_proj[:, None, :], grid_rows, grid_cols)[:, 0].astype(jnp.bfloat16)
    starting = (
        jnp.full((heads_here, tokens_here), -jnp.inf, jnp.float32),
        jnp.zeros((heads_here, tokens_here), jnp.float32),
        jnp.zeros((tokens_here, heads_here, VDIM), jnp.float32),
    )
    key_piece = lax.all_gather(expanded, "sp", axis=0, tiled=True)
    rope_piece = lax.all_gather(rope_key, "sp", axis=0, tiled=True)
    piece_rows = key_piece.shape[0]
    key_block = math.gcd(piece_rows, 1024)
    split_heads = key_piece.reshape(piece_rows, heads_here, NOPE + VDIM)

    def one_block(turn_index, state):
        row_max, row_sum, running_out = state
        offset = turn_index * key_block
        block_keys = lax.dynamic_slice_in_dim(split_heads, offset, key_block, 0)
        block_rope = lax.dynamic_slice_in_dim(rope_piece, offset, key_block, 0)
        scores = jnp.einsum(
            "thd,jhd->htj", query_nope, block_keys[..., :NOPE], preferred_element_type=jnp.float32
        )
        scores = scores + jnp.einsum(
            "thd,jd->htj", query_rope, block_rope, preferred_element_type=jnp.float32
        )
        new_max = jnp.maximum(row_max, jnp.max(scores, axis=-1))
        rescale = jnp.exp(row_max - new_max)
        weights = jnp.exp(scores - new_max[..., None])
        row_sum = row_sum * rescale + jnp.sum(weights, axis=-1)
        running_out = running_out * rescale.T[..., None] + jnp.einsum(
            "htj,jhd->thd",
            weights.astype(jnp.bfloat16),
            block_keys[..., NOPE:],
            preferred_element_type=jnp.float32,
        )
        return (new_max, row_sum, running_out)

    row_max, row_sum, running_out = lax.fori_loop(0, piece_rows // key_block, one_block, starting)
    attended = (
        (running_out / row_sum.T[..., None])
        .astype(jnp.bfloat16)
        .reshape(tokens_here, heads_here * VDIM)
    )
    log_weight_sum = row_max + jnp.log(row_sum)
    conv_mixed = conv_branch(gate_proj, pre_proj, value_proj, conv_kernel)
    mixed = lax.psum_scatter(
        (
            jnp.dot(attended, output_attend, preferred_element_type=jnp.float32)
            + jnp.dot(conv_mixed, output_conv, preferred_element_type=jnp.float32)
        ).astype(jnp.bfloat16),
        "tp",
        scatter_dimension=0,
        tiled=True,
    )
    return (mixed, log_weight_sum)


def solution(mesh):
    return jax.shard_map(
        body,
        mesh=mesh,
        in_specs=(
            P("sp", "tp"),
            P(),
            P(None, "tp"),
            P(None, "tp"),
            P(),
            P(),
            P(None, "tp"),
            P(None, "tp"),
            P(None, "tp"),
            P(None, "tp"),
            P(None, "tp"),
            P("tp", None),
            P("tp", None),
        ),
        out_specs=(P(("sp", "tp"), None), P("tp", "sp")),
        check_vma=False,
    )
```

profile of v0, /device:TPU:0, one launch (start us, length us, event | category | flops | bytes accessed | tf_op | source)
XLA Modules:
  0.0 135.6 jit_solution(17453811287171782455)
XLA Ops:
  7.2 0.0 copy-start
  7.2 0.0 copy-start.5
  7.2 0.0 copy-start.1
  7.2 0.0 copy-start.3
  7.2 0.0 copy-start.4
  7.2 0.0 all-gather.3.cloned.1.call-start
  7.3 0.7 all-gather.3.cloned.1.call-update
  8.0 0.0 reduce-scatter.2.cloned.1.call-start
  8.0 1.0 multiply_reduce_fusion
  9.0 1.2 copy.19
  10.3 1.3 copy.20
  11.5 1.2 copy.21
  12.8 15.2 %psum.7 = f32[256,1]{0,1:T(1,128)S(1)} all-reduce(f32[256,1]{0,1:T(1,128)S(1)} %bitcast.73), channel_id=1, replica_groups=mesh['sp'=4,'tp'=8] {'tp'}, use_global_device_ids=true, to_apply=%region_1.0 | all-reduce | flops 256 | bytes 2048 | tf_op jit(solution)/shard_map/psum | solution.py:82
  28.0 0.0 copy-done.5
  28.0 0.6 slice_bitcast_fusion.13
  28.6 0.0 copy-done.1
  28.6 0.9 constant_dynamic-update-slice_fusion.5
  29.5 0.0 copy-done.3
  29.6 0.7 constant_dynamic-update-slice_fusion.4
  30.3 0.7 constant_dynamic-update-slice_fusion.3
  31.0 0.8 constant_dynamic-update-slice_fusion.2
  31.8 0.9 constant_dynamic-update-slice_fusion.1
  32.7 0.8 constant_dynamic-update-slice_fusion
  33.5 2.7 %all-gather.3.cloned.1.call-done = bf16[256,2048]{1,0:T(8,128)(2,1)} async-done(((bf16[256,256]{1,0:T(8,128)(2,1)}), bf16[256,2048]{1,0:T(8,128)(2,1)}) %all-gather.3.cloned.1.call-update) | async-done | bytes 1048592 | tf_op jit(solution)/shard_map/all_gather | solution.py:84
  36.2 3.1 %convolution_multiply_fusion = f32[256,704]{0,1:T(8,128)S(1)} fusion(bf16[2048,704]{0,1:T(8,128)(2,1)} %constant_dynamic-update-slice_fusion, bf16[256,2048]{1,0:T(8,128)(2,1)} %all-gather.3.cloned.1.call-done, f32[2048]{0:T(1024)S(1)} %copy-done.7, f32[256]{0:T(256)S(1)} %bitcast.74), kind=kOutput, calls=%fused_computation.6 | convolution fusion | flops 739950592 | bytes 4662272 | tf_op jit(solution)/shard_map/dot_general | solution.py:86
  39.4 0.1 constant_dynamic-update-slice_fusion.9
  39.6 0.1 constant_dynamic-update-slice_fusion.8
  39.7 0.2 fusion.52
  39.9 13.4 %all-gather = bf16[1024,1,64]{0,2,1:T(8,128)(2,1)S(1)} all-gather(bf16[256,1,64]{0,2,1:T(8,128)(2,1)S(1)} %pad_maximum_fusion), channel_id=2, replica_groups=mesh['sp'=4,'tp'=8] {'sp'}, dimensions={0}, use_global_device_ids=true | all-gather | bytes 163840 | tf_op jit(solution)/shard_map/all_gather | solution.py:126
  53.4 0.1 constant_dynamic-update-slice_fusion.6
  53.5 9.3 %all_gather.13 = bf16[256,512]{0,1:T(8,128)(2,1)S(1)} all-gather(bf16[256,64]{0,1:T(8,128)(2,1)S(1)} %slice.196), channel_id=1, replica_groups=mesh['sp'=4,'tp'=8] {'tp'}, dimensions={1}, use_global_device_ids=true | all-gather | bytes 294912 | tf_op jit(solution)/shard_map/all_gather | solution.py:108
  62.8 0.1 fusion.10
  62.9 0.4 convolution_convert_fusion
  63.3 16.1 %all_gather.14 = bf16[1024,256]{1,0:T(8,128)(2,1)S(1)} all-gather(bf16[256,256]{1,0:T(8,128)(2,1)S(1)} %convolution_convert_fusion), channel_id=1, replica_groups=mesh['sp'=4,'tp'=8] {'sp'}, dimensions={0}, use_global_device_ids=true | all-gather | bytes 655360 | tf_op jit(solution)/shard_map/all_gather | solution.py:125
  79.4 0.3 convolution_bitcast_fusion.1
  79.7 0.4 fusion.66
  80.2 0.3 fusion.7
  80.5 0.1 fusion.65
  80.5 3.7 %collective-permute-start = (bf16[1,128]{0,1:T(8,128)(2,1)S(1)}, bf16[1,128]{0,1:T(8,128)(2,1)S(1)}, u32[]{:S(2)}, u32[]{:S(2)}) collective-permute-start(bf16[1,128]{0,1:T(8,128)(2,1)S(1)} %get-tuple-element.26), channel_id=1, source_target_pairs={{0,8},{8,16},{16,24},{1,9},{9,17},{17,25},{2,10},{10,18},{18,26},{... | collective-permute-start | bytes 776 | tf_op jit(solution)/shard_map/ppermute | solution.py:23
  84.2 1.3 collective-permute-start.1
  85.5 2.4 %fusion.9 = f32[256,2048]{1,0:T(8,128)} fusion(bf16[128,2048]{1,0:T(8,128)(2,1)S(1)} %copy-done, f32[1,256,1024]{2,1,0:T(8,128)S(1)} %get-tuple-element.44, f32[256]{0:T(256)S(1)} %get-tuple-element.43, bf16[1024,1,256]{2,0,1:T(8,128)(2,1)S(1)} %bitcast.70, f32[256]{0:T(256)S(1)} %get-tuple-element.42, f32[256]{0:T(256)S(1)} %get-tuple-element.41), kind=kOutput, calls=%fused_computation.19 | convolution fusion | flops 201949184 | bytes 3935232 | tf_op jit(solution)/shard_map/dot_general | solution.py:164
  88.0 0.0 collective-permute-done
  88.0 2.1 %collective-permute-done.1 = bf16[1,128]{0,1:T(8,128)(2,1)S(1)} collective-permute-done((bf16[1,128]{0,1:T(8,128)(2,1)S(1)}, bf16[1,128]{0,1:T(8,128)(2,1)S(1)}, u32[]{:S(2)}, u32[]{:S(2)}) %collective-permute-start.1) | collective-permute-done | bytes 288 | tf_op jit(solution)/shard_map/ppermute | solution.py:24
  90.0 0.1 maximum_convert_fusion
  90.2 3.2 %fusion = bf16[256,2048]{1,0:T(8,128)(2,1)} fusion(f32[256,2048]{1,0:T(8,128)} %fusion.9, bf16[128,2048]{1,0:T(8,128)(2,1)S(1)} %copy-done.2, f32[258,128]{0,1:T(8,128)S(1)} %maximum_convert_fusion, f32[256,704]{0,1:T(8,128)S(1)} %convolution_multiply_fusion, f32[128]{0:T(128)} %get-tuple-element.38, f32[128]{0:T(128)} %get-tuple-element.39, ...), kind=kOutput, calls=%fused_computation.1 | convolution fusion | flops 135495680 | bytes 4195840 | tf_op jit(solution)/shard_map/dot_general | solution.py:165
  93.4 0.0 reduce-scatter.2.cloned.1.call-update
  93.4 0.6 log_add_fusion
  94.0 34.8 %reduce-scatter.2.cloned.1.call-done = bf16[32,2048]{1,0:T(8,128)(2,1)} async-done(((bf16[256,2048]{1,0:T(8,128)(2,1)}), bf16[32,2048]{1,0:T(8,128)(2,1)}) %reduce-scatter.2.cloned.1.call-update) | async-done | bytes 131088 | tf_op jit(solution)/shard_map/reduce_scatter | solution.py:162
  (23 shorter events, 0.1 us)
Async XLA Ops:
  7.2 78.4 %copy-start = (bf16[128,2048]{1,0:T(8,128)(2,1)S(1)}, bf16[128,2048]{1,0:T(8,128)(2,1)}, u32[]{:S(2)}) copy-start(bf16[128,2048]{1,0:T(8,128)(2,1)} %param.24) | copy-start | bytes 1572868
  7.2 20.8 %copy-start.5 = (bf16[3,128]{1,0:T(4,128)(2,1)S(1)}, bf16[3,128]{1,0:T(4,128)(2,1)}, u32[]{:S(2)}) copy-start(bf16[3,128]{1,0:T(4,128)(2,1)} %param.23) | copy-start | bytes 2308
  7.2 21.4 %copy-start.1 = (bf16[2048,192]{0,1:T(8,128)(2,1)S(1)}, bf16[2048,192]{0,1:T(8,128)(2,1)}, u32[]{:S(2)}) copy-start(bf16[2048,192]{0,1:T(8,128)(2,1)} %param.15) | copy-start | bytes 2359300
  7.2 22.3 %copy-start.3 = (bf16[2048,64]{0,1:T(8,128)(2,1)S(1)}, bf16[2048,64]{0,1:T(8,128)(2,1)}, u32[]{:S(2)}) copy-start(bf16[2048,64]{0,1:T(8,128)(2,1)} %param.16) | copy-start | bytes 786436
  7.2 23.1 %copy-start.4 = (bf16[2048,64]{0,1:T(8,128)(2,1)S(1)}, bf16[2048,64]{0,1:T(8,128)(2,1)}, u32[]{:S(2)}) copy-start(bf16[2048,64]{0,1:T(8,128)(2,1)} %param.17) | copy-start | bytes 786436
  7.2 29.0 %all-gather.3.cloned.1.call-start = ((), (), s32[]{:S(2)}) async-start(), calls=%async_computation.1 | async-start | bytes 1179648 | tf_op jit(solution)/shard_map/all_gather | solution.py:84
  8.0 120.8 %reduce-scatter.2.cloned.1.call-start = ((), (), s32[]{:S(2)}) async-start(), calls=%async_computation.2 | async-start | bytes 1179648 | tf_op jit(solution)/shard_map/reduce_scatter | solution.py:162
  28.6 7.6 %copy-start.7 = (f32[2048]{0:T(1024)S(1)}, f32[2048]{0:T(1024)}, u32[]{:S(2)}) copy-start(f32[2048]{0:T(1024)} %param.14) | copy-start | bytes 24580
  36.2 26.7 %copy-start.6 = (bf16[512,256]{1,0:T(8,128)(2,1)S(1)}, bf16[512,256]{1,0:T(8,128)(2,1)}, u32[]{:S(2)}) copy-start(bf16[512,256]{1,0:T(8,128)(2,1)} %param.19) | copy-start | bytes 786436
  36.2 26.7 %copy-start.8 = (f32[512]{0:T(512)S(1)}, f32[512]{0:T(512)}, u32[]{:S(2)}) copy-start(f32[512]{0:T(512)} %param.18) | copy-start | bytes 6148
  80.1 10.0 %copy-start.2 = (bf16[128,2048]{1,0:T(8,128)(2,1)S(1)}, bf16[128,2048]{1,0:T(8,128)(2,1)}, u32[]{:S(2)}) copy-start(bf16[128,2048]{1,0:T(8,128)(2,1)} %param.25) | copy-start | bytes 1572868
  80.5 7.4 %collective-permute-start = (bf16[1,128]{0,1:T(8,128)(2,1)S(1)}, bf16[1,128]{0,1:T(8,128)(2,1)S(1)}, u32[]{:S(2)}, u32[]{:S(2)}) collective-permute-start(bf16[1,128]{0,1:T(8,128)(2,1)S(1)} %get-tuple-element.26), channel_id=1, source_target_pairs={{0,8},{8,16},{16,24},{1,9},{9,17},{17,25},{2,10},{10,18},{18,26},{... | collective-permute-start | bytes 776 | tf_op jit(solution)/shard_map/ppermute | solution.py:23
  84.2 5.8 %collective-permute-start.1 = (bf16[1,128]{0,1:T(8,128)(2,1)S(1)}, bf16[1,128]{0,1:T(8,128)(2,1)S(1)}, u32[]{:S(2)}, u32[]{:S(2)}) collective-permute-start(bf16[1,128]{0,1:T(8,128)(2,1)S(1)} %get-tuple-element.36), channel_id=1, source_target_pairs={{8,0},{16,8},{24,16},{9,1},{17,9},{25,17},{10,2},{18,10},{26,18},{... | collective-permute-start | bytes 776 | tf_op jit(solution)/shard_map/ppermute | solution.py:24
Sparse Core Ops, SparseCore 0:
  9.9 26.2 all-gather.2
  93.5 35.1 reduce-scatter.1
where the time goes:
time: 136 us
  blocking collectives  53.9 us (40%)
  waiting for transfers between devices  40.2 us (30%)
  between operations  14.3 us (11%)
  matrix products  9.9 us (7%)
  local copies, waits for them, and re-layouts  9.39 us (7%)
  starting transfers between devices  5.04 us (4%)
  other arithmetic  2.83 us (2%)
    reduce_scatter x1, waiting for transfers between devices, body(): lax.psum_scatter((jnp.dot(attended, output_attend, preferred_element_type...  34.8 us
    all_gather x1, blocking collectives, body(): key_piece = lax.all_gather(expanded, 'sp', axis=0, tiled=True)  16.1 us
    psum x1, blocking collectives, body(): lax.psum(jnp.sum(inputs_f32 * inputs_f32, axis=1, keepdims=True), 'tp')  15.2 us
    all_gather x1, blocking collectives, body(): rope_piece = lax.all_gather(rope_key, 'sp', axis=0, tiled=True)  13.4 us
    all_gather x1, blocking collectives, body(): lax.all_gather(latent_proj.astype(jnp.bfloat16), 'tp', axis=1, tiled=True)  9.26 us
    unnamed x27, local copies, waits for them, and re-layouts  7.86 us
    ppermute x1, starting transfers between devices, with_halo(): before = lax.ppermute(last, axis, up)  3.67 us
    dot_general x1, matrix products, body(): jnp.dot(conv_mixed, output_conv, preferred_element_type=jnp.float32)  3.22 us
  transfers between devices with their start and end apart: 4, of which 3 were waited for; matrix products, arithmetic and copies ran while one was open for 10% of the time, Pallas kernels for 0%

commit v1 on v0

--- a/solution.py
+++ b/solution.py
@@ -122,8 +122,11 @@
         jnp.zeros((heads_here, tokens_here), jnp.float32),
         jnp.zeros((tokens_here, heads_here, VDIM), jnp.float32),
     )
-    key_piece = lax.all_gather(expanded, "sp", axis=0, tiled=True)
-    rope_piece = lax.all_gather(rope_key, "sp", axis=0, tiled=True)
+    key_piece, rope_piece = jnp.split(
+        lax.all_gather(jnp.concatenate([expanded, rope_key], axis=1), "sp", axis=0, tiled=True),
+        [expanded.shape[1]],
+        axis=1,
+    )
     piece_rows = key_piece.shape[0]
     key_block = math.gcd(piece_rows, 1024)
     split_heads = key_piece.reshape(piece_rows, heads_here, NOPE + VDIM)

time: 136 us -> 123 us (0.904)
  blocking collectives: 53.9 us -> 42.5 us
    all_gather x2 -> x1, blocking collectives: 29.5 us -> 18.1 us  [body(): lax.all_gather(jnp.concatenate([expanded, rope_key], axis=1), 'sp', axis=...]
  transfers between devices with their start and end apart: 4 -> 4, of which waited for: 3 -> 3; matrix products, arithmetic and copies ran while one was open for 10% -> 11% of each run, Pallas kernels for 0% -> 0%
where the time goes in v1:
time: 123 us
  blocking collectives  42.5 us (35%)
  waiting for transfers between devices  40.2 us (33%)
  between operations  14.3 us (12%)
  matrix products  9.9 us (8%)
  local copies, waits for them, and re-layouts  9.46 us (8%)
  starting transfers between devices  3.75 us (3%)
  other arithmetic  2.86 us (2%)
    reduce_scatter x1, waiting for transfers between devices, body(): lax.psum_scatter((jnp.dot(attended, output_attend, preferred_element_type...  34.8 us
    all_gather x1, blocking collectives, body(): lax.all_gather(jnp.concatenate([expanded, rope_key], axis=1), 'sp', axis=...  18.1 us
    psum x1, blocking collectives, body(): lax.psum(jnp.sum(inputs_f32 * inputs_f32, axis=1, keepdims=True), 'tp')  15.2 us
    all_gather x1, blocking collectives, body(): lax.all_gather(latent_proj.astype(jnp.bfloat16), 'tp', axis=1, tiled=True)  9.27 us
    unnamed x27, local copies, waits for them, and re-layouts  7.89 us
    dot_general x1, matrix products, body(): jnp.dot(conv_mixed, output_conv, preferred_element_type=jnp.float32)  3.22 us
    dot_general x1, matrix products, body(): running = jnp.dot(scaled, joined, preferred_element_type=jnp.float32)  3.12 us
    all_gather x1, waiting for transfers between devices, body(): lax.all_gather(activations, 'tp', axis=1, tiled=True).astype(jnp.float32)  2.65 us
  transfers between devices with their start and end apart: 4, of which 3 were waited for; matrix products, arithmetic and copies ran while one was open for 11% of the time, Pallas kernels for 0%

profile of v1, /device:TPU:0, one launch (start us, length us, event | category | flops | bytes accessed | tf_op | source)
XLA Modules:
  0.0 123.0 jit_solution(8662854067318313465)
XLA Ops:
  7.2 0.0 copy-start
  7.2 0.0 copy-start.5
  7.2 0.0 copy-start.1
  7.2 0.0 copy-start.3
  7.2 0.0 copy-start.4
  7.2 0.0 all-gather.2.cloned.1.call-start
  7.3 0.7 all-gather.2.cloned.1.call-update
  8.0 0.0 reduce-scatter.2.cloned.1.call-start
  8.0 1.0 multiply_reduce_fusion
  9.0 1.2 %copy.19 = bf16[2048,128]{0,1:T(8,128)(2,1)S(1)} copy(bf16[2048,128]{1,0:T(8,128)(2,1)} %param.20) | data formatting | bytes 1048576 | tf_op args[7]
  10.3 1.3 %copy.20 = bf16[2048,128]{0,1:T(8,128)(2,1)S(1)} copy(bf16[2048,128]{1,0:T(8,128)(2,1)} %param.21) | data formatting | bytes 1048576 | tf_op args[8]
  11.5 1.2 %copy.21 = bf16[2048,128]{0,1:T(8,128)(2,1)S(1)} copy(bf16[2048,128]{1,0:T(8,128)(2,1)} %param.22) | data formatting | bytes 1048576 | tf_op args[9]
  12.8 15.2 %psum.7 = f32[256,1]{0,1:T(1,128)S(1)} all-reduce(f32[256,1]{0,1:T(1,128)S(1)} %bitcast.69), channel_id=1, replica_groups=mesh['sp'=4,'tp'=8] {'tp'}, use_global_device_ids=true, to_apply=%region_1.0 | all-reduce | flops 256 | bytes 2048 | tf_op jit(solution)/shard_map/psum | solution.py:82
  28.0 0.0 copy-done.5
  28.0 0.6 slice_bitcast_fusion.14
  28.6 0.0 copy-done.1
  28.6 0.9 constant_dynamic-update-slice_fusion.5
  29.5 0.0 copy-done.3
  29.6 0.7 constant_dynamic-update-slice_fusion.4
  30.3 0.0 copy-done.4
  30.3 0.7 constant_dynamic-update-slice_fusion.3
  31.0 0.8 constant_dynamic-update-slice_fusion.2
  31.8 0.9 constant_dynamic-update-slice_fusion.1
  32.7 0.8 constant_dynamic-update-slice_fusion
  33.5 2.6 %all-gather.2.cloned.1.call-done = bf16[256,2048]{1,0:T(8,128)(2,1)} async-done(((bf16[256,256]{1,0:T(8,128)(2,1)}), bf16[256,2048]{1,0:T(8,128)(2,1)}) %all-gather.2.cloned.1.call-update) | async-done | bytes 1048592 | tf_op jit(solution)/shard_map/all_gather | solution.py:84
  36.2 3.1 %convolution_multiply_fusion = f32[256,704]{0,1:T(8,128)S(1)} fusion(bf16[2048,704]{0,1:T(8,128)(2,1)} %constant_dynamic-update-slice_fusion, bf16[256,2048]{1,0:T(8,128)(2,1)} %all-gather.2.cloned.1.call-done, f32[2048]{0:T(1024)S(1)} %copy-done.7, f32[256]{0:T(256)S(1)} %bitcast.70), kind=kOutput, calls=%fused_computation.6 | convolution fusion | flops 739950592 | bytes 4662272 | tf_op jit(solution)/shard_map/dot_general | solution.py:86
  39.4 0.1 constant_dynamic-update-slice_fusion.9
  39.6 0.1 constant_dynamic-update-slice_fusion.8
  39.7 9.3 %all_gather.10 = bf16[256,512]{0,1:T(8,128)(2,1)S(1)} all-gather(bf16[256,64]{0,1:T(8,128)(2,1)S(1)} %slice.196), channel_id=1, replica_groups=mesh['sp'=4,'tp'=8] {'tp'}, dimensions={1}, use_global_device_ids=true | all-gather | bytes 294912 | tf_op jit(solution)/shard_map/all_gather | solution.py:108
  49.0 0.1 fusion.10
  49.1 0.1 constant_dynamic-update-slice_fusion.7
  49.2 0.2 fusion.52
  49.5 0.4 convolution_convert_fusion
  49.9 18.1 %all_gather.11 = bf16[1024,320]{0,1:T(8,128)(2,1)S(1)} all-gather(bf16[256,320]{0,1:T(8,128)(2,1)S(1)} %pad_maximum_fusion), channel_id=1, replica_groups=mesh['sp'=4,'tp'=8] {'sp'}, dimensions={0}, use_global_device_ids=true | all-gather | bytes 819200 | tf_op jit(solution)/shard_map/all_gather | solution.py:126
  68.1 0.3 convolution_bitcast_fusion.1
  68.4 0.4 fusion.66
  68.8 0.3 fusion.7
  69.1 0.1 fusion.65
  69.2 2.4 %collective-permute-start = (bf16[1,128]{0,1:T(8,128)(2,1)S(1)}, bf16[1,128]{0,1:T(8,128)(2,1)S(1)}, u32[]{:S(2)}, u32[]{:S(2)}) collective-permute-start(bf16[1,128]{0,1:T(8,128)(2,1)S(1)} %get-tuple-element.26), channel_id=1, source_target_pairs={{0,8},{8,16},{16,24},{1,9},{9,17},{17,25},{2,10},{10,18},{18,26},{... | collective-permute-start | bytes 776 | tf_op jit(solution)/shard_map/ppermute | solution.py:23
  71.6 1.3 %collective-permute-start.1 = (bf16[1,128]{0,1:T(8,128)(2,1)S(1)}, bf16[1,128]{0,1:T(8,128)(2,1)S(1)}, u32[]{:S(2)}, u32[]{:S(2)}) collective-permute-start(bf16[1,128]{0,1:T(8,128)(2,1)S(1)} %get-tuple-element.36), channel_id=1, source_target_pairs={{8,0},{16,8},{24,16},{9,1},{17,9},{25,17},{10,2},{18,10},{26,18},{... | collective-permute-start | bytes 776 | tf_op jit(solution)/shard_map/ppermute | solution.py:24
  72.9 2.4 %fusion.9 = f32[256,2048]{1,0:T(8,128)} fusion(bf16[128,2048]{1,0:T(8,128)(2,1)S(1)} %copy-done, f32[1,256,1024]{2,1,0:T(8,128)S(1)} %get-tuple-element.44, f32[256]{0:T(256)S(1)} %get-tuple-element.43, bf16[1024,1,256]{0,2,1:T(8,128)(2,1)S(1)} %slice_bitcast_fusion, f32[256]{0:T(256)S(1)} %get-tuple-element.42, f32[256]{0:T(256)S(1)} %get-tuple-element.41), kind=kOutput, calls=%fused_computation.19 | convolution fusion | flops 201949184 | bytes 3935232 | tf_op jit(solution)/shard_map/dot_general | solution.py:167
  75.3 0.0 collective-permute-done
  75.4 2.1 %collective-permute-done.1 = bf16[1,128]{0,1:T(8,128)(2,1)S(1)} collective-permute-done((bf16[1,128]{0,1:T(8,128)(2,1)S(1)}, bf16[1,128]{0,1:T(8,128)(2,1)S(1)}, u32[]{:S(2)}, u32[]{:S(2)}) %collective-permute-start.1) | collective-permute-done | bytes 288 | tf_op jit(solution)/shard_map/ppermute | solution.py:24
  77.4 0.1 maximum_convert_fusion
  77.5 3.2 %fusion = bf16[256,2048]{1,0:T(8,128)(2,1)} fusion(f32[256,2048]{1,0:T(8,128)} %fusion.9, bf16[128,2048]{1,0:T(8,128)(2,1)S(1)} %copy-done.2, f32[258,128]{0,1:T(8,128)S(1)} %maximum_convert_fusion, f32[256,704]{0,1:T(8,128)S(1)} %convolution_multiply_fusion, f32[128]{0:T(128)} %get-tuple-element.38, f32[128]{0:T(128)} %get-tuple-element.39, ...), kind=kOutput, calls=%fused_computation.1 | convolution fusion | flops 135495680 | bytes 4195840 | tf_op jit(solution)/shard_map/dot_general | solution.py:168
  80.8 0.0 reduce-scatter.2.cloned.1.call-update
  80.8 0.6 log_add_fusion
  81.4 34.8 %reduce-scatter.2.cloned.1.call-done = bf16[32,2048]{1,0:T(8,128)(2,1)} async-done(((bf16[256,2048]{1,0:T(8,128)(2,1)}), bf16[32,2048]{1,0:T(8,128)(2,1)}) %reduce-scatter.2.cloned.1.call-update) | async-done | bytes 131088 | tf_op jit(solution)/shard_map/reduce_scatter | solution.py:165
  (24 shorter events, 0.2 us)
Async XLA Ops:
  7.2 65.7 %copy-start = (bf16[128,2048]{1,0:T(8,128)(2,1)S(1)}, bf16[128,2048]{1,0:T(8,128)(2,1)}, u32[]{:S(2)}) copy-start(bf16[128,2048]{1,0:T(8,128)(2,1)} %param.24) | copy-start | bytes 1572868
  7.2 20.8 %copy-start.5 = (bf16[3,128]{1,0:T(4,128)(2,1)S(1)}, bf16[3,128]{1,0:T(4,128)(2,1)}, u32[]{:S(2)}) copy-start(bf16[3,128]{1,0:T(4,128)(2,1)} %param.23) | copy-start | bytes 2308
  7.2 21.4 %copy-start.1 = (bf16[2048,192]{0,1:T(8,128)(2,1)S(1)}, bf16[2048,192]{0,1:T(8,128)(2,1)}, u32[]{:S(2)}) copy-start(bf16[2048,192]{0,1:T(8,128)(2,1)} %param.15) | copy-start | bytes 2359300
  7.2 22.3 %copy-start.3 = (bf16[2048,64]{0,1:T(8,128)(2,1)S(1)}, bf16[2048,64]{0,1:T(8,128)(2,1)}, u32[]{:S(2)}) copy-start(bf16[2048,64]{0,1:T(8,128)(2,1)} %param.16) | copy-start | bytes 786436
  7.2 23.1 %copy-start.4 = (bf16[2048,64]{0,1:T(8,128)(2,1)S(1)}, bf16[2048,64]{0,1:T(8,128)(2,1)}, u32[]{:S(2)}) copy-start(bf16[2048,64]{0,1:T(8,128)(2,1)} %param.17) | copy-start | bytes 786436
  7.2 29.0 %all-gather.2.cloned.1.call-start = ((), (), s32[]{:S(2)}) async-start(), calls=%async_computation.1 | async-start | bytes 1179648 | tf_op jit(solution)/shard_map/all_gather | solution.py:84
  8.0 108.2 %reduce-scatter.2.cloned.1.call-start = ((), (), s32[]{:S(2)}) async-start(), calls=%async_computation.2 | async-start | bytes 1179648 | tf_op jit(solution)/shard_map/reduce_scatter | solution.py:165
  28.6 7.6 %copy-start.7 = (f32[2048]{0:T(1024)S(1)}, f32[2048]{0:T(1024)}, u32[]{:S(2)}) copy-start(f32[2048]{0:T(1024)} %param.14) | copy-start | bytes 24580
  36.2 13.3 %copy-start.6 = (bf16[512,256]{1,0:T(8,128)(2,1)S(1)}, bf16[512,256]{1,0:T(8,128)(2,1)}, u32[]{:S(2)}) copy-start(bf16[512,256]{1,0:T(8,128)(2,1)} %param.19) | copy-start | bytes 786436
  36.2 13.3 %copy-start.8 = (f32[512]{0:T(512)S(1)}, f32[512]{0:T(512)}, u32[]{:S(2)}) copy-start(f32[512]{0:T(512)} %param.18) | copy-start | bytes 6148
  68.8 8.7 %copy-start.2 = (bf16[128,2048]{1,0:T(8,128)(2,1)S(1)}, bf16[128,2048]{1,0:T(8,128)(2,1)}, u32[]{:S(2)}) copy-start(bf16[128,2048]{1,0:T(8,128)(2,1)} %param.25) | copy-start | bytes 1572868
  69.2 6.1 %collective-permute-start = (bf16[1,128]{0,1:T(8,128)(2,1)S(1)}, bf16[1,128]{0,1:T(8,128)(2,1)S(1)}, u32[]{:S(2)}, u32[]{:S(2)}) collective-permute-start(bf16[1,128]{0,1:T(8,128)(2,1)S(1)} %get-tuple-element.26), channel_id=1, source_target_pairs={{0,8},{8,16},{16,24},{1,9},{9,17},{17,25},{2,10},{10,18},{18,26},{... | collective-permute-start | bytes 776 | tf_op jit(solution)/shard_map/ppermute | solution.py:23
  71.6 5.8 %collective-permute-start.1 = (bf16[1,128]{0,1:T(8,128)(2,1)S(1)}, bf16[1,128]{0,1:T(8,128)(2,1)S(1)}, u32[]{:S(2)}, u32[]{:S(2)}) collective-permute-start(bf16[1,128]{0,1:T(8,128)(2,1)S(1)} %get-tuple-element.36), channel_id=1, source_target_pairs={{8,0},{16,8},{24,16},{9,1},{17,9},{25,17},{10,2},{18,10},{26,18},{... | collective-permute-start | bytes 776 | tf_op jit(solution)/shard_map/ppermute | solution.py:24
Sparse Core Ops, SparseCore 0:
  9.9 26.2 all-gather.1
  80.9 35.2 reduce-scatter.1
